TPU v7x, 32 devices: a whole 2x2x4 slice. The times are simulated.
32 devices in a mesh: sp: 4 (over x, core), dp: 8 (over z, y).
Axes of the slice: x: 2, y: 2, z: 4, core: 2. Of those that a mesh axis runs over, the one named last changes fastest.
Arguments:
- tokens: bfloat16 [8, 1536, 2048], P('dp', 'sp'), may hold values from -6 to 6
- w_value: bfloat16 [2048, 1024], P('dp'), may hold values from -0.125 to 0.125
- w_gate: bfloat16 [2048, 1024], P('dp'), may hold values from -0.125 to 0.125
- conv_taps: bfloat16 [31, 1024], replicated, may hold values from -1 to 1
- norm_gain: bfloat16 [1024], replicated, may hold values from 0.099609375 to 1.8984375
- w_out: bfloat16 [1024, 2048], P(None, 'dp'), may hold values from -0.1875 to 0.1875
Outputs:
- mixed: bfloat16 [8, 1536, 2048], P('dp', 'sp')
All inputs are finite; a program needn't handle non-finite values.
Results may differ from a plain program's by a relative error of at most 0.013.
Values may be sent and summed in bfloat16 or wider, within the bound.
No kernel may reach another device: no remote copies, remote signals or barrier semaphores. Data moves between devices by JAX's collectives and lax.ppermute only.
A program may use at most 64 MiB of HBM per device.

v0:
```python
import jax
import jax.numpy as jnp
from jax import lax
from jax.sharding import PartitionSpec as P

EPSILON = 1e-06


def passed_along(x, axis, by):
    length = lax.axis_size(axis)
    pairs = [(i, i + by) for i in range(length) if 0 <= i + by < length]
    return lax.ppermute(x, axis, pairs)


def depthwise_conv(signal, local_taps, left_pad):
    kernel_form = jnp.transpose(local_taps)[:, None, :]
    result = lax.conv_general_dilated(
        signal[None],
        kernel_form,
        (1,),
        [(left_pad, 0)],
        dimension_numbers=("NCH", "OIH", "NCH"),
        feature_group_count=signal.shape[0],
        preferred_element_type=jnp.float32,
    )
    return result[0].astype(jnp.bfloat16)


def body(tokens, w_value, w_gate, conv_taps, norm_gain, w_out):
    seq_rows = tokens[0]
    tok_count = seq_rows.shape[0]
    kernel_len = conv_taps.shape[0]
    value_sum = jnp.einsum(
        "dc,td->ct",
        lax.all_gather(w_value, "dp", axis=0, tiled=True),
        seq_rows,
        preferred_element_type=jnp.float32,
    )
    gate_sum = jnp.einsum(
        "dc,td->ct",
        lax.all_gather(w_gate, "dp", axis=0, tiled=True),
        seq_rows,
        preferred_element_type=jnp.float32,
    )
    gated = (value_sum * jax.nn.sigmoid(gate_sum)).astype(jnp.bfloat16)
    last_rows = gated[:, tok_count - (kernel_len - 1) :]
    earlier = passed_along(last_rows, "sp", 1)
    extended = jnp.concatenate([earlier, gated], axis=1)
    conv_out = depthwise_conv(extended, conv_taps, 0)
    wide = conv_out.astype(jnp.float32)
    chan_mean = jnp.mean(wide, 0, keepdims=True)
    centred = wide - chan_mean
    chan_var = jnp.mean(centred * centred, 0, keepdims=True)
    normed = centred * lax.rsqrt(chan_var + EPSILON) * norm_gain.astype(jnp.float32)[:, None]
    activated = (normed * jax.nn.sigmoid(normed)).astype(jnp.bfloat16)
    projected = jnp.einsum(
        "ct,cd->td",
        activated,
        lax.all_gather(w_out, "dp", axis=1, tiled=True),
        preferred_element_type=jnp.float32,
    ).astype(jnp.bfloat16)
    return projected[None]


def solution(mesh):
    placed = (P("dp", "sp", None), P("dp", None), P("dp", None), P(), P(), P(None, "dp"))
    return jax.shard_map(
        body, mesh=mesh, in_specs=placed, out_specs=P("dp", "sp", None), check_vma=False
    )
```

profile of v0, /device:TPU:0, one launch (start us, length us, event | category | flops | bytes accessed | tf_op | source)
XLA Modules:
  0.0 246.4 jit_solution(6799378059922831921)
XLA Ops:
  6.5 0.0 copy-start
  6.5 0.0 all-gather.6.cloned.1.call-start
  6.5 0.7 all-gather.6.cloned.1.call-update
  7.3 0.0 all-gather.4.cloned.1.call-start
  7.3 0.7 all-gather.4.cloned.1.call-update
  8.0 0.0 all-gather.8.cloned.1.call-start
  8.1 0.7 all-gather.8.cloned.1.call-update
  8.7 76.3 %all-gather.6.cloned.1.call-done = bf16[2048,1024]{1,0:T(8,128)(2,1)} async-done(((bf16[256,1024]{1,0:T(8,128)(2,1)}), bf16[2048,1024]{1,0:T(8,128)(2,1)}) %all-gather.6.cloned.1.call-update) | async-done | bytes 4194320 | tf_op jit(solution)/shard_map/all_gather | solution.py:41
  85.0 0.0 copy-done
  85.0 4.0 %fusion.4 = f32[1024,384]{0,1:T(8,128)S(1)} fusion(bf16[2048,1024]{1,0:T(8,128)(2,1)} %all-gather.6.cloned.1.call-done, bf16[1,384,2048]{2,1,0:T(8,128)(2,1)S(1)} %copy-done), kind=kOutput, calls=%fused_computation.8 | convolution fusion | flops 1610612736 | bytes 7340032 | tf_op jit(solution)/shard_map/dc,td->ct/dot_general | solution.py:39
  89.0 0.0 copy-start.1
  89.0 69.5 %all-gather.4.cloned.1.call-done = bf16[2048,1024]{1,0:T(8,128)(2,1)} async-done(((bf16[256,1024]{1,0:T(8,128)(2,1)}), bf16[2048,1024]{1,0:T(8,128)(2,1)}) %all-gather.4.cloned.1.call-update) | async-done | bytes 4194320 | tf_op jit(solution)/shard_map/all_gather | solution.py:35
  158.5 4.1 %multiply_convert_fusion.1 = bf16[1024,384]{0,1:T(8,128)(2,1)S(1)} fusion(f32[1024,384]{0,1:T(8,128)S(1)} %fusion.4, bf16[2048,1024]{1,0:T(8,128)(2,1)} %all-gather.4.cloned.1.call-done, bf16[1,384,2048]{2,1,0:T(8,128)(2,1)S(1)} %copy-done), kind=kOutput, calls=%fused_computation.12 | convolution fusion | flops 1612578816 | bytes 8126464 | tf_op jit(solution)/shard_map/dc,td->ct/dot_general | solution.py:33
  162.6 1.3 collective-permute-start
  163.9 0.0 copy-done.1
  163.9 0.9 collective-permute-done
  164.8 0.2 maximum_bitcast_fusion
  165.0 0.1 pad
  165.0 0.2 reshape.17
  165.2 0.0 copy-start.2
  165.2 0.0 copy-start.3
  165.2 0.5 copy.12
  165.7 0.1 slice.7
  165.8 0.2 copy-done.2
  166.0 0.0 copy-done.3
  166.0 3.8 %fusion.17 = f32[8,52,1024]{2,0,1:T(8,128)S(1)} fusion(bf16[1024,1,7,30]{0,2,3,1:T(8,128)(2,1)S(1)} %slice.7, bf16[1024,1,8,52]{0,2,3,1:T(8,128)(2,1)S(1)} %copy.12, pred[8,52]{0,1:T(8,128)(4,1)S(1)} %copy-done.3, bf16[1024,1,31]{0,2,1:T(8,128)(2,1)S(1)} %bitcast.35), kind=kOutput, calls=%fused_computation.20 | convolution fusion | flops 31719424 | bytes 3049888 | tf_op jit(solution)/shard_map/conv_general_dilated | solution.py:17
  169.8 2.2 copy.14
  172.1 1.6 reshape.21
  173.7 0.2 slice_reduce_fusion
  173.8 0.3 multiply_reduce_fusion
  174.1 60.3 %all-gather.8.cloned.1.call-done = bf16[1024,2048]{1,0:T(8,128)(2,1)} async-done(((bf16[1024,256]{1,0:T(8,128)(2,1)}), bf16[1024,2048]{1,0:T(8,128)(2,1)}) %all-gather.8.cloned.1.call-update) | async-done | bytes 4194320 | tf_op jit(solution)/shard_map/all_gather | solution.py:59
  234.5 5.5 %fusion.1 = bf16[1,384,2048]{2,1,0:T(8,128)(2,1)} fusion(bf16[1024,2048]{1,0:T(8,128)(2,1)} %all-gather.8.cloned.1.call-done, f32[1,416,1024]{2,1,0:T(8,128)S(1)} %reshape.21, f32[1024]{0:T(1024)S(1)} %convert_element_type.26, f32[384]{0:T(512)S(1)} %add_rsqrt_fusion, f32[384]{0:T(512)S(1)} %broadcast_multiply_fusion), kind=kOutput, calls=%fused_computation.3 | convolution fusion | flops 1614544896 | bytes 7348224 | tf_op jit(solution)/shard_map/ct,cd->td/dot_general | solution.py:56
  (4 shorter events, 0.0 us)
Async XLA Ops:
  6.5 78.5 %copy-start = (bf16[1,384,2048]{2,1,0:T(8,128)(2,1)S(1)}, bf16[1,384,2048]{2,1,0:T(8,128)(2,1)}, u32[]{:S(2)}) copy-start(bf16[1,384,2048]{2,1,0:T(8,128)(2,1)} %param.6) | copy-start | bytes 4718596
  6.5 78.5 %all-gather.6.cloned.1.call-start = ((), (), s32[]{:S(2)}) async-start(), calls=%async_computation.1 | async-start | bytes 4718592 | tf_op jit(solution)/shard_map/all_gather | solution.py:41
  7.3 151.2 %all-gather.4.cloned.1.call-start = ((), (), s32[]{:S(2)}) async-start(), calls=%async_computation | async-start | bytes 4718592 | tf_op jit(solution)/shard_map/all_gather | solution.py:35
  8.0 226.4 %all-gather.8.cloned.1.call-start = ((), (), s32[]{:S(2)}) async-start(), calls=%async_computation.2 | async-start | bytes 4718592 | tf_op jit(solution)/shard_map/all_gather | solution.py:59
  89.0 74.9 %copy-start.1 = (bf16[1024]{0:T(1024)(128)(2,1)S(1)}, bf16[1024]{0:T(1024)(128)(2,1)}, u32[]{:S(2)}) copy-start(bf16[1024]{0:T(1024)(128)(2,1)} %param.10) | copy-start | bytes 6148
  162.6 2.2 collective-permute-start
  165.2 0.8 copy-start.2
  165.2 0.8 copy-start.3
Sparse Core Ops, SparseCore 0:
  9.5 75.5 all-gather.5
  87.1 71.3 all-gather.3
  160.5 73.8 all-gather.7
where the time goes:
time: 247 us; the launch traced here: 246 us
  waiting for transfers between devices  209 us (85%)
  matrix products  17.3 us (7%)
  between operations  13.2 us (5%)
  local copies, waits for them, and re-layouts  4.87 us (2%)
    all_gather x1, waiting for transfers between devices, body(): lax.all_gather(w_gate, 'dp', axis=0, tiled=True)  76.3 us
    all_gather x1, waiting for transfers between devices, body(): lax.all_gather(w_value, 'dp', axis=0, tiled=True)  69.5 us
    all_gather x1, waiting for transfers between devices, body(): lax.all_gather(w_out, 'dp', axis=1, tiled=True)  60.3 us
    dot_general x1, matrix products, body(): jnp.einsum('ct,cd->td', activated, lax.all_gather(w_out, 'dp', axis=1, ti...  5.46 us
  transfers between devices with their start and end apart: 4, of which 4 were waited for; matrix products, arithmetic and copies ran while one was open for 7% of the time, Pallas kernels for 0%

commit v1 on v0

--- a/solution.py
+++ b/solution.py
@@ -4,6 +4,24 @@
 from jax.sharding import PartitionSpec as P
 
 EPSILON = 1e-06
+
+
+def ring_apply(x, axis, dim, apply, out_dim):
+    size, here, rows = (lax.axis_size(axis), lax.axis_index(axis), x.shape[dim])
+    upward = [(i, (i + 1) % size) for i in range(size)]
+    current, out = (x, None)
+    for step in range(size):
+        owner = (here - step) % size
+        coming = lax.ppermute(current, axis, upward) if step < size - 1 else None
+        made = apply(current, owner * rows)
+        length = made.shape[out_dim]
+        if out is None:
+            out = jnp.zeros(
+                (*made.shape[:out_dim], size * length, *made.shape[out_dim + 1 :]), made.dtype
+            )
+        out = lax.dynamic_update_slice_in_dim(out, made, owner * length, axis=out_dim)
+        current = coming
+    return out
 
 
 def passed_along(x, axis, by):
@@ -53,11 +71,14 @@
     chan_var = jnp.mean(centred * centred, 0, keepdims=True)
     normed = centred * lax.rsqrt(chan_var + EPSILON) * norm_gain.astype(jnp.float32)[:, None]
     activated = (normed * jax.nn.sigmoid(normed)).astype(jnp.bfloat16)
-    projected = jnp.einsum(
-        "ct,cd->td",
-        activated,
-        lax.all_gather(w_out, "dp", axis=1, tiled=True),
-        preferred_element_type=jnp.float32,
+    projected = ring_apply(
+        w_out,
+        "dp",
+        1,
+        lambda own_block, at: jnp.einsum(
+            "ct,cd->td", activated, own_block, preferred_element_type=jnp.float32
+        ),
+        1,
     ).astype(jnp.bfloat16)
     return projected[None]
 

time: 247 us -> 234 us (0.947)
  waiting for transfers between devices: 209 us -> 182 us
  local copies, waits for them, and re-layouts: 4.87 us -> 10.6 us
  starting transfers between devices: 1.37 us -> 6.27 us
    ppermute x0 -> x7, waiting for transfers between devices: none -> 113 us  [ring_apply(): coming = lax.ppermute(current, axis, upward) if step < size - 1 else None]
    all_gather x1, waiting for transfers between devices: 76.3 us -> 0.01 us  [body(): lax.all_gather(w_gate, 'dp', axis=0, tiled=True)]
    all_gather x1 -> x0, waiting for transfers between devices: 60.3 us -> none  [body(): lax.all_gather(w_out, 'dp', axis=1, tiled=True)]
    unnamed x8 -> x32, local copies, waits for them, and re-layouts: 0.25 us -> 5.81 us
    ppermute x0 -> x7, starting transfers between devices: none -> 4.94 us  [ring_apply(): coming = lax.ppermute(current, axis, upward) if step < size - 1 else None]
    dot_general x1 -> x8, matrix products: 5.46 us -> 5.09 us  [body(): jnp.einsum('ct,cd->td', activated, own_block, preferred_element_type=jnp....]
  transfers between devices with their start and end apart: 4 -> 10, of which waited for: 4 -> 7; matrix products, arithmetic and copies ran while one was open for 7% -> 10% of each run, Pallas kernels for 0% -> 0%
where the time goes in v1:
time: 234 us; the launch traced here: 233 us
  waiting for transfers between devices  182 us (78%)
  matrix products  18.8 us (8%)
  between operations  13.8 us (6%)
  local copies, waits for them, and re-layouts  10.6 us (5%)
  starting transfers between devices  6.27 us (3%)
    ppermute x7, waiting for transfers between devices, ring_apply(): coming = lax.ppermute(current, axis, upward) if step < size - 1 else None  113 us
    all_gather x1, waiting for transfers between devices, body(): lax.all_gather(w_value, 'dp', axis=0, tiled=True)  67.6 us
    unnamed x32, local copies, waits for them, and re-layouts  5.81 us
    dot_general x1, matrix products, body(): jnp.einsum('dc,td->ct', lax.all_gather(w_gate, 'dp', axis=0, tiled=True),...  5.38 us
    dot_general x8, matrix products, body(): jnp.einsum('ct,cd->td', activated, own_block, preferred_element_type=jnp....  5.09 us
    ppermute x7, starting transfers between devices, ring_apply(): coming = lax.ppermute(current, axis, upward) if step < size - 1 else None  4.94 us
  transfers between devices with their start and end apart: 10, of which 7 were waited for; matrix products, arithmetic and copies ran while one was open for 10% of the time, Pallas kernels for 0%

profile of v1, /device:TPU:0, one launch (start us, length us, event | category | flops | bytes accessed | tf_op | source)
XLA Modules:
  0.0 232.7 jit_solution(2550943828507368246)
XLA Ops:
  6.5 0.7 all-gather.5.cloned.1.call-update
  7.3 0.7 all-gather.3.cloned.1.call-update
  8.0 3.0 %collective-permute-start.1 = (bf16[1024,256]{1,0:T(8,128)(2,1)}, bf16[1024,256]{1,0:T(8,128)(2,1)S(1)}, u32[]{:S(2)}, u32[]{:S(2)}) collective-permute-start(bf16[1024,256]{1,0:T(8,128)(2,1)} %param.11), channel_id=1, source_target_pairs={{0,1},{1,2},{2,3},{3,4},{4,5},{5,6},{6,7},{7,0},{8,9},{9,10},{10,1... | collective-permute-start | bytes 1572872 | tf_op jit(solution)/shard_map/ppermute | solution.py:15
  11.1 15.5 %collective-permute-done.1 = bf16[1024,256]{1,0:T(8,128)(2,1)S(1)} collective-permute-done((bf16[1024,256]{1,0:T(8,128)(2,1)}, bf16[1024,256]{1,0:T(8,128)(2,1)S(1)}, u32[]{:S(2)}, u32[]{:S(2)}) %collective-permute-start.1) | collective-permute-done | bytes 524320 | tf_op jit(solution)/shard_map/ppermute | solution.py:15
  26.6 0.9 copy-done.3
  27.5 1.1 collective-permute-start.2
  28.5 25.8 %collective-permute-done.2 = bf16[1024,256]{1,0:T(8,128)(2,1)S(1)} collective-permute-done((bf16[1024,256]{1,0:T(8,128)(2,1)S(1)}, bf16[1024,256]{1,0:T(8,128)(2,1)S(1)}, u32[]{:S(2)}, u32[]{:S(2)}) %collective-permute-start.2) | collective-permute-done | bytes 524320 | tf_op jit(solution)/shard_map/ppermute | solution.py:15
  54.4 0.8 copy-done.5
  55.2 27.0 %collective-permute-done.3 = bf16[1024,256]{1,0:T(8,128)(2,1)S(1)} collective-permute-done((bf16[1024,256]{1,0:T(8,128)(2,1)S(1)}, bf16[1024,256]{1,0:T(8,128)(2,1)S(1)}, u32[]{:S(2)}, u32[]{:S(2)}) %collective-permute-start.3) | collective-permute-done | bytes 524320 | tf_op jit(solution)/shard_map/ppermute | solution.py:15
  82.2 0.8 copy-done.7
  83.0 26.9 %collective-permute-done.4 = bf16[1024,256]{1,0:T(8,128)(2,1)S(1)} collective-permute-done((bf16[1024,256]{1,0:T(8,128)(2,1)S(1)}, bf16[1024,256]{1,0:T(8,128)(2,1)S(1)}, u32[]{:S(2)}, u32[]{:S(2)}) %collective-permute-start.4) | collective-permute-done | bytes 524320 | tf_op jit(solution)/shard_map/ppermute | solution.py:15
  109.8 0.8 copy-done.9
  110.6 16.7 %collective-permute-done.5 = bf16[1024,256]{1,0:T(8,128)(2,1)S(1)} collective-permute-done((bf16[1024,256]{1,0:T(8,128)(2,1)S(1)}, bf16[1024,256]{1,0:T(8,128)(2,1)S(1)}, u32[]{:S(2)}, u32[]{:S(2)}) %collective-permute-start.5) | collective-permute-done | bytes 524320 | tf_op jit(solution)/shard_map/ppermute | solution.py:15
  127.4 5.4 %fusion.3 = f32[1024,384]{0,1:T(8,128)} fusion(bf16[2048,1024]{1,0:T(8,128)(2,1)} %all-gather.5.cloned.1.call-done, bf16[1,384,2048]{2,1,0:T(8,128)(2,1)S(1)} %copy-done), kind=kOutput, calls=%fused_computation.6 | convolution fusion | flops 1610612736 | bytes 7340032 | tf_op jit(solution)/shard_map/dc,td->ct/dot_general | solution.py:57
  132.7 67.6 %all-gather.3.cloned.1.call-done = bf16[2048,1024]{1,0:T(8,128)(2,1)} async-done(((bf16[256,1024]{1,0:T(8,128)(2,1)}), bf16[2048,1024]{1,0:T(8,128)(2,1)}) %all-gather.3.cloned.1.call-update) | async-done | bytes 4194320 | tf_op jit(solution)/shard_map/all_gather | solution.py:53
  200.4 4.5 %multiply_convert_fusion.1 = bf16[1024,384]{0,1:T(8,128)(2,1)S(1)} fusion(f32[1024,384]{0,1:T(8,128)} %fusion.3, bf16[2048,1024]{1,0:T(8,128)(2,1)} %all-gather.3.cloned.1.call-done, bf16[1,384,2048]{2,1,0:T(8,128)(2,1)S(1)} %copy-done), kind=kOutput, calls=%fused_computation.11 | convolution fusion | flops 1612578816 | bytes 8126464 | tf_op jit(solution)/shard_map/dc,td->ct/dot_general | solution.py:51
  204.9 1.3 collective-permute-start
  206.5 0.8 collective-permute-start.7
  207.7 0.5 copy.12
  208.5 3.8 %fusion.16 = f32[8,52,1024]{2,0,1:T(8,128)S(1)} fusion(bf16[1024,1,7,30]{0,2,3,1:T(8,128)(2,1)S(1)} %slice.7, bf16[1024,1,8,52]{0,2,3,1:T(8,128)(2,1)S(1)} %copy.12, pred[8,52]{0,1:T(8,128)(4,1)S(1)} %copy-done.15, bf16[1024,1,31]{0,2,1:T(8,128)(2,1)S(1)} %bitcast.50), kind=kOutput, calls=%fused_computation.27 | convolution fusion | flops 31719424 | bytes 3049888 | tf_op jit(solution)/shard_map/conv_general_dilated | solution.py:35
  212.3 2.3 copy.14
  214.6 1.6 reshape.21
  216.7 0.6 multiply_convert_fusion
  217.7 0.4 convolution_dynamic-update-slice_fusion.7
  218.3 0.4 convolution_dynamic-update-slice_fusion.6
  218.8 0.4 convolution_dynamic-update-slice_fusion.5
  219.9 0.4 convolution_dynamic-update-slice_fusion.3
  220.5 0.4 convolution_dynamic-update-slice_fusion.2
  220.9 1.4 convolution_dynamic-update-slice_fusion.1
  222.3 1.0 collective-permute-done.7
  223.3 1.4 convolution_dynamic-update-slice_fusion
  224.7 1.1 copy-done.1
  (48 shorter events, 3.0 us)
Async XLA Ops:
  6.5 120.8 %copy-start = (bf16[1,384,2048]{2,1,0:T(8,128)(2,1)S(1)}, bf16[1,384,2048]{2,1,0:T(8,128)(2,1)}, u32[]{:S(2)}) copy-start(bf16[1,384,2048]{2,1,0:T(8,128)(2,1)} %param.6) | copy-start | bytes 4718596
  6.5 120.8 %all-gather.5.cloned.1.call-start = ((), (), s32[]{:S(2)}) async-start(), calls=%async_computation.1 | async-start | bytes 4718592 | tf_op jit(solution)/shard_map/all_gather | solution.py:59
  7.3 193.1 %all-gather.3.cloned.1.call-start = ((), (), s32[]{:S(2)}) async-start(), calls=%async_computation | async-start | bytes 4718592 | tf_op jit(solution)/shard_map/all_gather | solution.py:53
  8.0 18.6 %collective-permute-start.1 = (bf16[1024,256]{1,0:T(8,128)(2,1)}, bf16[1024,256]{1,0:T(8,128)(2,1)S(1)}, u32[]{:S(2)}, u32[]{:S(2)}) collective-permute-start(bf16[1024,256]{1,0:T(8,128)(2,1)} %param.11), channel_id=1, source_target_pairs={{0,1},{1,2},{2,3},{3,4},{4,5},{5,6},{6,7},{7,0},{8,9},{9,10},{10,1... | collective-permute-start | bytes 1572872 | tf_op jit(solution)/shard_map/ppermute | solution.py:15
  26.6 0.9 copy-start.3
  27.5 26.9 %collective-permute-start.2 = (bf16[1024,256]{1,0:T(8,128)(2,1)S(1)}, bf16[1024,256]{1,0:T(8,128)(2,1)S(1)}, u32[]{:S(2)}, u32[]{:S(2)}) collective-permute-start(bf16[1024,256]{1,0:T(8,128)(2,1)S(1)} %collective-permute-done.1), channel_id=1, source_target_pairs={{0,1},{1,2},{2,3},{3,4},{4,5},{5,6},{6,7},{7,0},{8,9},{9,10},{10,1... | collective-permute-start | bytes 1572872 | tf_op jit(solution)/shard_map/ppermute | solution.py:15
  54.4 0.8 copy-start.5
  55.2 27.0 %collective-permute-start.3 = (bf16[1024,256]{1,0:T(8,128)(2,1)S(1)}, bf16[1024,256]{1,0:T(8,128)(2,1)S(1)}, u32[]{:S(2)}, u32[]{:S(2)}) collective-permute-start(bf16[1024,256]{1,0:T(8,128)(2,1)S(1)} %collective-permute-done.2), channel_id=1, source_target_pairs={{0,1},{1,2},{2,3},{3,4},{4,5},{5,6},{6,7},{7,0},{8,9},{9,10},{10,1... | collective-permute-start | bytes 1572872 | tf_op jit(solution)/shard_map/ppermute | solution.py:15
  82.1 0.8 copy-start.7
  82.9 26.9 %collective-permute-start.4 = (bf16[1024,256]{1,0:T(8,128)(2,1)S(1)}, bf16[1024,256]{1,0:T(8,128)(2,1)S(1)}, u32[]{:S(2)}, u32[]{:S(2)}) collective-permute-start(bf16[1024,256]{1,0:T(8,128)(2,1)S(1)} %collective-permute-done.3), channel_id=1, source_target_pairs={{0,1},{1,2},{2,3},{3,4},{4,5},{5,6},{6,7},{7,0},{8,9},{9,10},{10,1... | collective-permute-start | bytes 1572872 | tf_op jit(solution)/shard_map/ppermute | solution.py:15
  109.8 0.8 copy-start.9
  110.6 16.7 %collective-permute-start.5 = (bf16[1024,256]{1,0:T(8,128)(2,1)S(1)}, bf16[1024,256]{1,0:T(8,128)(2,1)S(1)}, u32[]{:S(2)}, u32[]{:S(2)}) collective-permute-start(bf16[1024,256]{1,0:T(8,128)(2,1)S(1)} %collective-permute-done.4), channel_id=1, source_target_pairs={{0,1},{1,2},{2,3},{3,4},{4,5},{5,6},{6,7},{7,0},{8,9},{9,10},{10,1... | collective-permute-start | bytes 1572872 | tf_op jit(solution)/shard_map/ppermute | solution.py:15
  127.3 5.4 %copy-start.11 = (bf16[1024,256]{1,0:T(8,128)(2,1)}, bf16[1024,256]{1,0:T(8,128)(2,1)S(1)}, u32[]{:S(2)}) copy-start(bf16[1024,256]{1,0:T(8,128)(2,1)S(1)} %collective-permute-done.5) | copy-start | bytes 1572868
  127.3 79.1 %collective-permute-start.6 = (bf16[1024,256]{1,0:T(8,128)(2,1)S(1)}, bf16[1024,256]{1,0:T(8,128)(2,1)}, u32[]{:S(2)}, u32[]{:S(2)}) collective-permute-start(bf16[1024,256]{1,0:T(8,128)(2,1)S(1)} %collective-permute-done.5), channel_id=1, source_target_pairs={{0,1},{1,2},{2,3},{3,4},{4,5},{5,6},{6,7},{7,0},{8,9},{9,10},{10,1... | collective-permute-start | bytes 1572872 | tf_op jit(solution)/shard_map/ppermute | solution.py:15
  132.7 73.6 %copy-start.13 = (bf16[1024]{0:T(1024)(128)(2,1)S(1)}, bf16[1024]{0:T(1024)(128)(2,1)}, u32[]{:S(2)}) copy-start(bf16[1024]{0:T(1024)(128)(2,1)} %param.10) | copy-start | bytes 6148
  204.9 2.3 collective-permute-start
  206.5 16.8 %collective-permute-start.7 = (bf16[1024,256]{1,0:T(8,128)(2,1)}, bf16[1024,256]{1,0:T(8,128)(2,1)}, u32[]{:S(2)}, u32[]{:S(2)}) collective-permute-start(bf16[1024,256]{1,0:T(8,128)(2,1)} %collective-permute-done.6), channel_id=1, source_target_pairs={{0,1},{1,2},{2,3},{3,4},{4,5},{5,6},{6,7},{7,0},{8,9},{9,10},{10,1... | collective-permute-start | bytes 1572872 | tf_op jit(solution)/shard_map/ppermute | solution.py:15
  207.7 0.8 copy-start.14
  207.7 0.8 copy-start.15
  216.6 1.1 copy-start.2
  217.2 1.1 copy-start.4
  217.7 1.1 copy-start.6
  218.3 1.1 copy-start.8
  218.8 1.1 copy-start.10
  219.4 1.1 copy-start.12
  224.7 1.1 copy-start.1
Sparse Core Ops, SparseCore 0:
  9.5 101.6 all-gather.4
  113.3 87.0 all-gather.2
